TPU v7x, 512 devices: a whole 4x8x8 slice. The times are simulated.
512 devices in a mesh: sp: 64 (over z, y), tp: 8 (over x, core).
Axes of the slice: x: 4, y: 8, z: 8, core: 2. Of those that a mesh axis runs over, the one named last changes fastest.
Arguments:
- latent: bfloat16 [16384, 2048], P(('sp', 'tp')), may hold values from -6 to 6
- context: bfloat16 [512, 2048], P('sp'), may hold values from -6 to 6
- condition: float32 [2048], P('tp'), may hold values from -6 to 6
- context_condition: float32 [2048], P('tp'), may hold values from -6 to 6
- modulation_weight: bfloat16 [2048, 6144], P('tp', 'sp'), may hold values from -0.125 to 0.125
- query_first: bfloat16 [2048, 512], P(None, 'tp'), may hold values from -1 to 1
- query_second: bfloat16 [2048, 512], P(None, 'tp'), may hold values from -1 to 1
- key_first: bfloat16 [2048, 512], P(None, 'tp'), may hold values from -1 to 1
- key_second: bfloat16 [2048, 512], P(None, 'tp'), may hold values from -1 to 1
- value_weight: bfloat16 [2048, 1024], P(None, 'tp'), may hold values from -0.125 to 0.125
- lambda_head: float32 [8], P('tp'), may hold values from 0.3 to 0.8
- context_score_boost: float32 [8], P('tp'), may hold values from 1.5 to 3
- head_gain: float32 [128], replicated, may hold values from 0.1 to 1.9
- output_weight: bfloat16 [1024, 2048], P('tp'), may hold values from -0.1875 to 0.1875
Outputs:
- updated: bfloat16 [16384, 2048], P(('sp', 'tp'))
All inputs are finite; a program needn't handle non-finite values.
Results may differ from a plain program's by a relative error of at most 0.0095.
Values may be sent and summed in bfloat16 or wider, within the bound.
A program may use at most 64 MiB of HBM per device.

v0:
```python
import jax
import jax.numpy as jnp
from jax import lax
from jax.sharding import PartitionSpec as P

HEAD_DIM = 64
VALUE_DIM = 128
GRID_W = 64
EPSILON = 1e-06
THETA = 10000.0
NEGATIVE = -1e30


def copy_for_each(shard, axis):
    size = lax.axis_size(axis)
    return lax.all_to_all(
        jnp.broadcast_to(shard[None], (size, *shard.shape)), axis, 0, 0, tiled=True
    )


def taken_together(shard, axis):
    return copy_for_each(shard, axis).sum(axis=0)


def joined_along(tiles, dim):
    tiles = jnp.moveaxis(tiles, 0, dim)
    lengths = tiles.shape
    return tiles.reshape(*lengths[:dim], lengths[dim] * lengths[dim + 1], *lengths[dim + 2 :])


def collect(shard, axis, dim):
    return joined_along(copy_for_each(shard, axis), dim)


def in_one_piece(arrays, axis, dim, along):
    widths = [a.shape[along] for a in arrays]
    both = jnp.concatenate(arrays, axis=along)
    out = lax.all_gather(both, axis, axis=dim, tiled=True)
    return tuple(jnp.split(out, [sum(widths[:k]) for k in range(1, len(widths))], axis=along))


def in_blocks(shard, dim, size):
    before, after = (shard.shape[:dim], shard.shape[dim + 1 :])
    return jnp.moveaxis(shard.reshape(*before, size, -1, *after), dim, 0)


def sum_at_owner(shard, axis, dim):
    tiles = in_blocks(shard, dim, lax.axis_size(axis))
    arrived = lax.all_to_all(tiles, axis, split_axis=0, concat_axis=0, tiled=True)
    return arrived.astype(jnp.float32).sum(axis=0)


def norm_rows(rows):
    values = rows.astype(jnp.float32)
    return values * lax.rsqrt(jnp.mean(values * values, axis=-1, keepdims=True) + EPSILON)


def rotate_pairs(values, positions):
    half = values.shape[-1] // 2
    quarter = half // 2
    reciprocal_norm = THETA ** (-jnp.arange(quarter, dtype=jnp.float32) / quarter)

    def turn(part, where):
        angle = where.astype(jnp.float32)[:, None] * reciprocal_norm[None, :]
        cosine_table = jnp.concatenate([jnp.cos(angle)] * 2, -1)[:, None, :]
        sine = jnp.concatenate([jnp.sin(angle)] * 2, -1)[:, None, :]
        flipped = jnp.concatenate([-part[..., quarter:], part[..., :quarter]], -1)
        return part * cosine_table + flipped * sine

    grid_row = positions // GRID_W
    grid_col = positions % GRID_W
    return jnp.concatenate(
        [turn(values[..., :half], grid_row), turn(values[..., half:], grid_col)], -1
    )


def block_extent(rows):
    size = min(rows, 1024)
    while rows % size:
        size -= 1
    return size


def body(
    latent,
    context,
    condition,
    context_condition,
    modulation_weight,
    query_first,
    query_second,
    key_first,
    key_second,
    value_weight,
    lambda_head,
    context_score_boost,
    head_gain,
    output_weight,
):
    width = latent.shape[1]
    signal = jax.nn.silu(jnp.stack([condition, context_condition])).astype(jnp.bfloat16)
    partial_mod = jnp.dot(signal, modulation_weight, preferred_element_type=jnp.float32)
    reduced = taken_together(partial_mod, "tp")
    modulation = collect(reduced, "sp", 1)
    shift = modulation[:, :width]
    scale = modulation[:, width : 2 * width]
    gate = modulation[:, 2 * width :]
    h_latent = (norm_rows(latent) * (1.0 + scale[0]) + shift[0]).astype(jnp.bfloat16)
    h_context = (norm_rows(context) * (1.0 + scale[1]) + shift[1]).astype(jnp.bfloat16)
    heads_dev = value_weight.shape[1] // VALUE_DIM
    span = heads_dev * HEAD_DIM
    offset = lax.axis_index("sp") * (latent.shape[0] * lax.axis_size("tp"))
    piece = collect(h_latent, "tp", 0)
    count = piece.shape[0]
    positions = offset + jnp.arange(count, dtype=jnp.int32)
    turned = []
    for weight in (query_first, query_second, key_first, key_second):
        product = jnp.dot(piece, weight, preferred_element_type=jnp.float32).reshape(
            count, heads_dev, HEAD_DIM
        )
        turned.append(rotate_pairs(product, positions).astype(jnp.bfloat16).reshape(count, span))
    values = jnp.dot(piece, value_weight, preferred_element_type=jnp.float32).astype(jnp.bfloat16)
    projected = jnp.concatenate(turned + [values], axis=1)
    queries = projected.shape[0]
    queries_one = projected[:, :span].reshape(queries, heads_dev, HEAD_DIM)
    queries_two = projected[:, span : 2 * span].reshape(queries, heads_dev, HEAD_DIM)
    latent_keys = projected[:, 2 * span : 4 * span]
    latent_values = projected[:, 4 * span :]

    def update(carry, block):
        keys_pair, values, boolean_markers = block
        count = keys_pair.shape[0]
        keys_one = keys_pair[:, :span].reshape(count, heads_dev, HEAD_DIM)
        keys_two = keys_pair[:, span:].reshape(count, heads_dev, HEAD_DIM)
        values_heads = values.reshape(count, heads_dev, VALUE_DIM)
        extra_score = context_score_boost[:, None, None] * boolean_markers[None, None, :]
        renewed = []
        for (highest, totals, weighted), query, keys in zip(
            carry, (queries_one, queries_two), (keys_one, keys_two)
        ):
            scores = (
                jnp.einsum("qhd,khd->hqk", query, keys, preferred_element_type=jnp.float32)
                * HEAD_DIM ** (-0.5)
                + extra_score
            )
            peak = jnp.maximum(highest, jnp.max(scores, axis=-1))
            exp_weights = jnp.exp(scores - peak[..., None])
            rescale = jnp.exp(highest - peak)
            totals = totals * rescale + jnp.sum(exp_weights, axis=-1)
            weighted = weighted * jnp.transpose(rescale)[:, :, None] + jnp.einsum(
                "hqk,khe->qhe",
                exp_weights.astype(jnp.bfloat16),
                values_heads,
                preferred_element_type=jnp.float32,
            )
            renewed.append((peak, totals, weighted))
        return (tuple(renewed), None)

    def fold_keys(carry, keys_pair, values, boolean_markers):
        rows = keys_pair.shape[0]
        size = block_extent(rows)
        count = rows // size
        blocks = (
            keys_pair.reshape(count, size, keys_pair.shape[1]),
            values.reshape(count, size, values.shape[1]),
            boolean_markers.reshape(count, size),
        )
        carry, unused = lax.scan(update, carry, blocks)
        return carry

    start_state = (
        jnp.full((heads_dev, queries), NEGATIVE, jnp.float32),
        jnp.zeros((heads_dev, queries), jnp.float32),
        jnp.zeros((queries, heads_dev, VALUE_DIM), jnp.float32),
    )
    initial = (start_state, start_state)
    keys_pair = jnp.concatenate(
        [
            jnp.dot(h_context, key_first, preferred_element_type=jnp.float32).astype(jnp.bfloat16),
            jnp.dot(h_context, key_second, preferred_element_type=jnp.float32).astype(jnp.bfloat16),
        ],
        axis=1,
    )
    values = jnp.dot(h_context, value_weight, preferred_element_type=jnp.float32).astype(
        jnp.bfloat16
    )
    all_keys, all_values = in_one_piece((keys_pair, values), "sp", 0, 1)
    carry = fold_keys(initial, all_keys, all_values, jnp.ones((all_keys.shape[0],), jnp.float32))
    pieces = (
        lax.all_gather(latent_keys, "sp", axis=0, tiled=True),
        lax.all_gather(latent_values, "sp", axis=0, tiled=True),
    )
    boolean_markers = jnp.zeros((pieces[0].shape[0],), jnp.float32)
    final = fold_keys(carry, pieces[0], pieces[1], boolean_markers)
    outcomes = [weighted / jnp.transpose(totals)[:, :, None] for highest, totals, weighted in final]
    mixed = outcomes[0] - lambda_head[None, :, None] * outcomes[1]
    normed = (
        mixed * lax.rsqrt(jnp.mean(mixed * mixed, axis=-1, keepdims=True) + EPSILON) * head_gain
    )
    heads_out = normed.astype(jnp.bfloat16).reshape(queries, heads_dev * VALUE_DIM)
    branch = sum_at_owner(
        jnp.dot(heads_out, output_weight, preferred_element_type=jnp.float32).astype(jnp.bfloat16),
        "tp",
        0,
    )
    return (latent.astype(jnp.float32) + gate[0] * branch).astype(jnp.bfloat16)


def solution(mesh):
    in_specs = (
        P(("sp", "tp"), None),
        P("sp", None),
        P("tp"),
        P("tp"),
        P("tp", "sp"),
        P(None, "tp"),
        P(None, "tp"),
        P(None, "tp"),
        P(None, "tp"),
        P(None, "tp"),
        P("tp"),
        P("tp"),
        P(),
        P("tp", None),
    )
    out_specs = P(("sp", "tp"), None)
    return jax.shard_map(body, mesh=mesh, in_specs=in_specs, out_specs=out_specs, check_vma=False)
```

profile of v0, /device:TPU:1, one launch (start us, length us, event | category | flops | bytes accessed | tf_op | source)
XLA Modules:
  0.0 344.7 jit_solution(9492942217073333725)
XLA Ops:
  6.5 1.1 fusion.88
  8.2 10.1 %all-to-all-start = ((f32[8,2,96]{2,1,0:T(2,128)}), f32[8,2,96]{2,1,0:T(2,128)S(1)}, u32[]{:S(2)}, u32[]{:S(2)}) async-start(f32[8,2,96]{2,1,0:T(2,128)} %broadcast_in_dim.22), calls=%async_computation | async-start | bytes 16384 | tf_op jit(solution)/shard_map/all_to_all | solution.py:16
  18.3 1.0 fusion.32
  19.3 3.6 %all-to-all-done = f32[8,2,96]{2,1,0:T(2,128)S(1)} async-done(((f32[8,2,96]{2,1,0:T(2,128)}), f32[8,2,96]{2,1,0:T(2,128)S(1)}, u32[]{:S(2)}, u32[]{:S(2)}) %all-to-all-start) | async-done | bytes 6176 | tf_op jit(solution)/shard_map/all_to_all | solution.py:16
  23.6 12.0 %all-to-all-start.1 = ((f32[64,2,96]{2,1,0:T(2,128)}), f32[64,2,96]{2,1,0:T(2,128)S(1)}, u32[]{:S(2)}, u32[]{:S(2)}) async-start(f32[64,2,96]{2,1,0:T(2,128)} %broadcast_in_dim.23), calls=%async_computation.1 | async-start | bytes 131072 | tf_op jit(solution)/shard_map/all_to_all | solution.py:16
  35.6 11.1 %all-to-all-done.1 = f32[64,2,96]{2,1,0:T(2,128)S(1)} async-done(((f32[64,2,96]{2,1,0:T(2,128)}), f32[64,2,96]{2,1,0:T(2,128)S(1)}, u32[]{:S(2)}, u32[]{:S(2)}) %all-to-all-start.1) | async-done | bytes 49184 | tf_op jit(solution)/shard_map/all_to_all | solution.py:16
  47.9 1.1 broadcast_in_dim.25
  49.0 5.7 %all-to-all-start.2 = ((bf16[8,32,2048]{2,1,0:T(8,128)(2,1)}), bf16[8,32,2048]{2,1,0:T(8,128)(2,1)S(1)}, u32[]{:S(2)}, u32[]{:S(2)}) async-start(bf16[8,32,2048]{2,1,0:T(8,128)(2,1)} %broadcast_in_dim.25), calls=%async_computation.2 | async-start | bytes 2097152 | tf_op jit(solution)/shard_map/all_to_all | solution.py:16
  55.0 14.8 %all-to-all-done.2 = bf16[8,32,2048]{2,1,0:T(8,128)(2,1)S(1)} async-done(((bf16[8,32,2048]{2,1,0:T(8,128)(2,1)}), bf16[8,32,2048]{2,1,0:T(8,128)(2,1)S(1)}, u32[]{:S(2)}, u32[]{:S(2)}) %all-to-all-start.2) | async-done | bytes 1048608 | tf_op jit(solution)/shard_map/all_to_all | solution.py:16
  71.4 1.1 convolution_convert_fusion.1
  74.8 35.7 %all_gather.9 = bf16[512,256]{1,0:T(8,128)(2,1)S(1)} all-gather(bf16[8,256]{1,0:T(8,128)(2,1)S(1)} %pad_maximum_fusion.5), channel_id=1, replica_groups=mesh['sp'=64,'tp'=8] {'sp'}, dimensions={0}, use_global_device_ids=true | all-gather | bytes 266240 | tf_op jit(solution)/shard_map/all_gather | solution.py:38
  113.4 35.7 %all-gather.3.cloned.1.call-done = bf16[16384,128]{0,1:T(8,128)(2,1)} async-done(((bf16[256,128]{0,1:T(8,128)(2,1)}), bf16[16384,128]{0,1:T(8,128)(2,1)}) %all-gather.3.cloned.1.call-update) | async-done | bytes 4194320 | tf_op jit(solution)/shard_map/all_gather | solution.py:190
  149.0 6.4 %copy.26 = bf16[16384,128]{1,0:T(8,128)(2,1)} copy(bf16[16384,128]{0,1:T(8,128)(2,1)} %all-gather.3.cloned.1.call-done) | data formatting | bytes 8388608 | tf_op jit(solution)/shard_map/while | solution.py:168
  155.4 79.0 %all-gather.5.cloned.1.call-done = bf16[16384,128]{1,0:T(8,128)(2,1)} async-done(((bf16[256,128]{1,0:T(8,128)(2,1)}), bf16[16384,128]{1,0:T(8,128)(2,1)}) %all-gather.5.cloned.1.call-update) | async-done | bytes 4194320 | tf_op jit(solution)/shard_map/all_gather | solution.py:191
  234.5 78.2 %while.4 = (s32[]{:T(128)}, f32[1,256]{1,0:T(1,128)S(1)}, f32[1,256]{1,0:T(1,128)S(1)}, f32[256,1,128]{0,2,1:T(8,128)S(1)}, f32[1,256]{1,0:T(1,128)S(1)}, /*inde...) while((s32[]{:T(128)}, f32[1,256]{1,0:T(1,128)S(1)}, ...), condition=%wide.region_12.13_spmd, body=%wide.region_7.12_spmd.sunk | while | flops 205128704 | bytes 8488073 | solution.py:168
  236.6 1.3 fusion.140
  238.0 1.3 fusion.139
  241.5 1.3 fusion.140
  242.9 1.3 fusion.139
  246.4 1.3 fusion.140
  247.8 1.3 fusion.139
  251.3 1.3 fusion.140
  252.6 1.3 fusion.139
  256.2 1.3 fusion.140
  257.5 1.3 fusion.139
  261.1 1.3 fusion.140
  262.4 1.3 fusion.139
  266.0 1.3 fusion.140
  267.3 1.3 fusion.139
  270.8 1.3 fusion.140
  272.2 1.3 fusion.139
  275.7 1.3 fusion.140
  277.1 1.3 fusion.139
  280.6 1.3 fusion.140
  281.9 1.3 fusion.139
  285.5 1.3 fusion.140
  286.8 1.3 fusion.139
  290.4 1.3 fusion.140
  291.7 1.3 fusion.139
  295.3 1.3 fusion.140
  296.6 1.3 fusion.139
  300.1 1.3 fusion.140
  301.5 1.3 fusion.139
  305.0 1.3 fusion.140
  306.4 1.3 fusion.139
  309.9 1.3 fusion.140
  311.2 1.3 fusion.139
  313.2 23.8 %all_to_all.20 = bf16[8,32,2048]{2,1,0:T(8,128)(2,1)S(1)} all-to-all(bf16[8,32,2048]{2,1,0:T(8,128)(2,1)S(1)} %bitcast.183), channel_id=1, replica_groups=mesh['sp'=64,'tp'=8] {'tp'}, dimensions={0} | all-to-all | bytes 2097152 | tf_op jit(solution)/shard_map/all_to_all | solution.py:49
  (229 shorter events, 44.0 us)
Async XLA Ops:
  6.5 306.2 %copy-start = (bf16[128,2048]{1,0:T(8,128)(2,1)S(1)}, bf16[128,2048]{1,0:T(8,128)(2,1)}, u32[]{:S(2)}) copy-start(bf16[128,2048]{1,0:T(8,128)(2,1)} %param.29) | copy-start | bytes 1572868
  6.5 63.2 %copy-start.3 = (bf16[2048,64]{0,1:T(8,128)(2,1)S(1)}, bf16[2048,64]{0,1:T(8,128)(2,1)}, u32[]{:S(2)}) copy-start(bf16[2048,64]{0,1:T(8,128)(2,1)} %param.23) | copy-start | bytes 786436
  6.5 63.7 %copy-start.4 = (bf16[2048,64]{0,1:T(8,128)(2,1)S(1)}, bf16[2048,64]{0,1:T(8,128)(2,1)}, u32[]{:S(2)}) copy-start(bf16[2048,64]{0,1:T(8,128)(2,1)} %param.24) | copy-start | bytes 786436
  6.5 64.9 %copy-start.1 = (bf16[2048,128]{1,0:T(8,128)(2,1)S(1)}, bf16[2048,128]{1,0:T(8,128)(2,1)}, u32[]{:S(2)}) copy-start(bf16[2048,128]{1,0:T(8,128)(2,1)} %param.25) | copy-start | bytes 1572868
  8.2 14.7 %all-to-all-start = ((f32[8,2,96]{2,1,0:T(2,128)}), f32[8,2,96]{2,1,0:T(2,128)S(1)}, u32[]{:S(2)}, u32[]{:S(2)}) async-start(f32[8,2,96]{2,1,0:T(2,128)} %broadcast_in_dim.22), calls=%async_computation | async-start | bytes 16384 | tf_op jit(solution)/shard_map/all_to_all | solution.py:16
  23.6 23.1 %all-to-all-start.1 = ((f32[64,2,96]{2,1,0:T(2,128)}), f32[64,2,96]{2,1,0:T(2,128)S(1)}, u32[]{:S(2)}, u32[]{:S(2)}) async-start(f32[64,2,96]{2,1,0:T(2,128)} %broadcast_in_dim.23), calls=%async_computation.1 | async-start | bytes 131072 | tf_op jit(solution)/shard_map/all_to_all | solution.py:16
  47.9 25.9 %copy-start.7 = (bf16[8,2048]{1,0:T(8,128)(2,1)S(1)}, bf16[8,2048]{1,0:T(8,128)(2,1)}, u32[]{:S(2)}) copy-start(bf16[8,2048]{1,0:T(8,128)(2,1)} %param.17) | copy-start | bytes 98308
  49.0 61.5 %copy-start.5 = (bf16[2048,64]{0,1:T(8,128)(2,1)S(1)}, bf16[2048,64]{0,1:T(8,128)(2,1)}, u32[]{:S(2)}) copy-start(bf16[2048,64]{0,1:T(8,128)(2,1)} %param.22) | copy-start | bytes 786436
  49.0 20.7 %all-to-all-start.2 = ((bf16[8,32,2048]{2,1,0:T(8,128)(2,1)}), bf16[8,32,2048]{2,1,0:T(8,128)(2,1)S(1)}, u32[]{:S(2)}, u32[]{:S(2)}) async-start(bf16[8,32,2048]{2,1,0:T(8,128)(2,1)} %broadcast_in_dim.25), calls=%async_computation.2 | async-start | bytes 2097152 | tf_op jit(solution)/shard_map/all_to_all | solution.py:16
  54.7 94.3 %all-gather.3.cloned.1.call-start = ((), (), s32[]{:S(2)}) async-start(), calls=%async_computation.4 | async-start | bytes 4259840 | tf_op jit(solution)/shard_map/all_gather | solution.py:190
  69.7 41.2 %copy-start.6 = (bf16[2048,64]{0,1:T(8,128)(2,1)S(1)}, bf16[2048,64]{0,1:T(8,128)(2,1)}, u32[]{:S(2)}) copy-start(bf16[2048,64]{0,1:T(8,128)(2,1)} %param.21) | copy-start | bytes 786436
  71.4 163.1 %all-gather.5.cloned.1.call-start = ((), (), s32[]{:S(2)}) async-start(), calls=%async_computation.5 | async-start | bytes 4259840 | tf_op jit(solution)/shard_map/all_gather | solution.py:191
  234.5 78.2 %copy-start.8 = (f32[128]{0:T(128)S(1)}, f32[128]{0:T(128)}, u32[]{:S(2)}) copy-start(f32[128]{0:T(128)} %param.28) | copy-start | bytes 1540
  312.6 24.6 %copy-start.2 = (bf16[32,2048]{1,0:T(8,128)(2,1)S(1)}, bf16[32,2048]{1,0:T(8,128)(2,1)}, u32[]{:S(2)}) copy-start(bf16[32,2048]{1,0:T(8,128)(2,1)} %param.16) | copy-start | bytes 393220
Sparse Core Ops, SparseCore 0:
  71.5 77.4 all-gather.2
  152.1 82.3 all-gather.4
where the time goes:
time: 347 us; the launch traced here: 345 us
  waiting for transfers between devices  144 us (41%)
  matrix products  60.3 us (17%)
  blocking collectives  59.5 us (17%)
  starting transfers between devices  27.8 us (8%)
  local copies, waits for them, and re-layouts  24.6 us (7%)
  between operations  14.9 us (4%)
  other arithmetic  12.3 us (4%)
    all_gather x1, waiting for transfers between devices, body(): lax.all_gather(latent_values, 'sp', axis=0, tiled=True)  79 us
    dot_general x34, matrix products, update(): jnp.einsum('hqk,khe->qhe', exp_weights.astype(jnp.bfloat16), values_heads...  43.2 us
    all_gather x1, blocking collectives, in_one_piece(): out = lax.all_gather(both, axis, axis=dim, tiled=True)  35.7 us
    all_gather x1, waiting for transfers between devices, body(): lax.all_gather(latent_keys, 'sp', axis=0, tiled=True)  35.7 us
    all_to_all x3, waiting for transfers between devices, copy_for_each(): lax.all_to_all(jnp.broadcast_to(shard[None], (size, *shard.shape)), axis,...  29.4 us
    all_to_all x3, starting transfers between devices, copy_for_each(): lax.all_to_all(jnp.broadcast_to(shard[None], (size, *shard.shape)), axis,...  27.8 us
    all_to_all x1, blocking collectives, sum_at_owner(): lax.all_to_all(tiles, axis, split_axis=0, concat_axis=0, tiled=True)  23.8 us
    squeeze x16, local copies, waits for them, and re-layouts, fold_keys(): carry, unused = lax.scan(update, carry, blocks)  15.6 us
  transfers between devices with their start and end apart: 5, of which 5 were waited for; matrix products, arithmetic and copies ran while one was open for 4% of the time, Pallas kernels for 0%

commit v1 on v0

--- a/solution.py
+++ b/solution.py
@@ -188,7 +188,9 @@
     carry = fold_keys(initial, all_keys, all_values, jnp.ones((all_keys.shape[0],), jnp.float32))
     pieces = (
         lax.all_gather(latent_keys, "sp", axis=0, tiled=True),
-        lax.all_gather(latent_values, "sp", axis=0, tiled=True),
+        jnp.concatenate(
+            lax.all_to_all(jnp.stack([latent_values] * lax.axis_size("sp")), "sp", 0, 0), axis=0
+        ),
     )
     boolean_markers = jnp.zeros((pieces[0].shape[0],), jnp.float32)
     final = fold_keys(carry, pieces[0], pieces[1], boolean_markers)

time: 347 us -> 371 us (1.069)
  blocking collectives: 59.5 us -> 186 us
  waiting for transfers between devices: 144 us -> 34.3 us
  starting transfers between devices: 27.8 us -> 33.5 us
    all_gather x1, blocking collectives: 35.7 us -> 161 us  [in_one_piece(): out = lax.all_gather(both, axis, axis=dim, tiled=True)]
    all_gather x1 -> x0, waiting for transfers between devices: 79 us -> none  [body(): lax.all_gather(latent_values, 'sp', axis=0, tiled=True)]
    all_gather x1, waiting for transfers between devices: 35.7 us -> 4.84 us  [body(): lax.all_gather(latent_keys, 'sp', axis=0, tiled=True)]
    all_to_all x0 -> x1, starting transfers between devices: none -> 5.79 us  [body(): lax.all_to_all(jnp.stack([latent_values] * lax.axis_size('sp')), 'sp', 0, 0)]
  transfers between devices with their start and end apart: 5 -> 5, of which waited for: 5 -> 4; matrix products, arithmetic and copies ran while one was open for 4% -> 4% of each run, Pallas kernels for 0% -> 0%
where the time goes in v1:
time: 371 us; the launch traced here: 369 us
  blocking collectives  186 us (50%)
  matrix products  59.7 us (16%)
  waiting for transfers between devices  34.3 us (9%)
  starting transfers between devices  33.5 us (9%)
  local copies, waits for them, and re-layouts  27.5 us (7%)
  between operations  14.9 us (4%)
  other arithmetic  12.3 us (3%)
    all_gather x1, blocking collectives, in_one_piece(): out = lax.all_gather(both, axis, axis=dim, tiled=True)  161 us
    dot_general x34, matrix products, update(): jnp.einsum('hqk,khe->qhe', exp_weights.astype(jnp.bfloat16), values_heads...  43.2 us
    all_to_all x3, waiting for transfers between devices, copy_for_each(): lax.all_to_all(jnp.broadcast_to(shard[None], (size, *shard.shape)), axis,...  29.4 us
    all_to_all x3, starting transfers between devices, copy_for_each(): lax.all_to_all(jnp.broadcast_to(shard[None], (size, *shard.shape)), axis,...  27.7 us
    all_to_all x1, blocking collectives, sum_at_owner(): lax.all_to_all(tiles, axis, split_axis=0, concat_axis=0, tiled=True)  25 us
    squeeze x16, local copies, waits for them, and re-layouts, fold_keys(): carry, unused = lax.scan(update, carry, blocks)  15.6 us
    dot_general x34, matrix products, update(): jnp.einsum('qhd,khd->hqk', query, keys, preferred_element_type=jnp.float32)  12 us
    reduce_sum x34, other arithmetic, update(): totals = totals * rescale + jnp.sum(exp_weights, axis=-1)  7.59 us
  transfers between devices with their start and end apart: 5, of which 4 were waited for; matrix products, arithmetic and copies ran while one was open for 4% of the time, Pallas kernels for 0%

profile of v1, /device:TPU:1, one launch (start us, length us, event | category | flops | bytes accessed | tf_op | source)
XLA Modules:
  0.0 368.9 jit_solution(741000447298736071)
XLA Ops:
  6.5 1.1 fusion.88
  8.2 10.1 %all-to-all-start = ((f32[8,2,96]{2,1,0:T(2,128)}), f32[8,2,96]{2,1,0:T(2,128)S(1)}, u32[]{:S(2)}, u32[]{:S(2)}) async-start(f32[8,2,96]{2,1,0:T(2,128)} %broadcast_in_dim.22), calls=%async_computation | async-start | bytes 16384 | tf_op jit(solution)/shard_map/all_to_all | solution.py:16
  18.3 1.0 fusion.32
  19.3 3.6 all-to-all-done
  23.6 12.0 %all-to-all-start.1 = ((f32[64,2,96]{2,1,0:T(2,128)}), f32[64,2,96]{2,1,0:T(2,128)S(1)}, u32[]{:S(2)}, u32[]{:S(2)}) async-start(f32[64,2,96]{2,1,0:T(2,128)} %broadcast_in_dim.23), calls=%async_computation.1 | async-start | bytes 131072 | tf_op jit(solution)/shard_map/all_to_all | solution.py:16
  35.6 11.1 %all-to-all-done.1 = f32[64,2,96]{2,1,0:T(2,128)S(1)} async-done(((f32[64,2,96]{2,1,0:T(2,128)}), f32[64,2,96]{2,1,0:T(2,128)S(1)}, u32[]{:S(2)}, u32[]{:S(2)}) %all-to-all-start.1) | async-done | bytes 49184 | tf_op jit(solution)/shard_map/all_to_all | solution.py:16
  47.9 1.1 broadcast_in_dim.25
  49.0 5.6 %all-to-all-start.2 = ((bf16[8,32,2048]{2,1,0:T(8,128)(2,1)}), bf16[8,32,2048]{2,1,0:T(8,128)(2,1)S(1)}, u32[]{:S(2)}, u32[]{:S(2)}) async-start(bf16[8,32,2048]{2,1,0:T(8,128)(2,1)} %broadcast_in_dim.25), calls=%async_computation.2 | async-start | bytes 2097152 | tf_op jit(solution)/shard_map/all_to_all | solution.py:16
  54.8 14.8 %all-to-all-done.2 = bf16[8,32,2048]{2,1,0:T(8,128)(2,1)S(1)} async-done(((bf16[8,32,2048]{2,1,0:T(8,128)(2,1)}), bf16[8,32,2048]{2,1,0:T(8,128)(2,1)S(1)}, u32[]{:S(2)}, u32[]{:S(2)}) %all-to-all-start.2) | async-done | bytes 1048608 | tf_op jit(solution)/shard_map/all_to_all | solution.py:16
  71.7 3.0 stack.11
  74.6 5.8 %all-to-all-start.3 = ((bf16[64,256,128]{2,1,0:T(8,128)(2,1)}), bf16[64,256,128]{2,1,0:T(8,128)(2,1)}, u32[]{:S(2)}, u32[]{:S(2)}) async-start(bf16[64,256,128]{2,1,0:T(8,128)(2,1)} %stack.11), calls=%async_computation.3 | async-start | bytes 8388608 | tf_op jit(solution)/shard_map/all_to_all | solution.py:192
  82.7 160.6 %all_gather.6 = bf16[512,256]{1,0:T(8,128)(2,1)S(1)} all-gather(bf16[8,256]{1,0:T(8,128)(2,1)S(1)} %pad_maximum_fusion.5), channel_id=1, replica_groups=mesh['sp'=64,'tp'=8] {'sp'}, dimensions={0}, use_global_device_ids=true | all-gather | bytes 266240 | tf_op jit(solution)/shard_map/all_gather | solution.py:38
  246.2 4.8 %all-gather.2.cloned.1.call-done = bf16[16384,128]{0,1:T(8,128)(2,1)} async-done(((bf16[256,128]{0,1:T(8,128)(2,1)}), bf16[16384,128]{0,1:T(8,128)(2,1)}) %all-gather.2.cloned.1.call-update) | async-done | bytes 4194320 | tf_op jit(solution)/shard_map/all_gather | solution.py:190
  251.0 6.4 %copy.26 = bf16[16384,128]{1,0:T(8,128)(2,1)} copy(bf16[16384,128]{0,1:T(8,128)(2,1)} %all-gather.2.cloned.1.call-done) | data formatting | bytes 8388608 | tf_op jit(solution)/shard_map/while | solution.py:168
  257.4 78.1 %while.4 = (s32[]{:T(128)}, f32[1,256]{1,0:T(1,128)S(1)}, f32[1,256]{1,0:T(1,128)S(1)}, f32[256,1,128]{0,2,1:T(8,128)S(1)}, f32[1,256]{1,0:T(1,128)S(1)}, /*inde...) while((s32[]{:T(128)}, f32[1,256]{1,0:T(1,128)S(1)}, ...), condition=%wide.region_12.13_spmd, body=%wide.region_7.12_spmd.sunk | while | flops 205128704 | bytes 8488073 | solution.py:168
  259.6 1.3 fusion.140
  260.9 1.3 fusion.139
  264.5 1.3 fusion.140
  265.8 1.3 fusion.139
  269.3 1.3 fusion.140
  270.7 1.3 fusion.139
  274.2 1.3 fusion.140
  275.6 1.3 fusion.139
  279.1 1.3 fusion.140
  280.5 1.3 fusion.139
  284.0 1.3 fusion.140
  285.3 1.3 fusion.139
  288.9 1.3 fusion.140
  290.2 1.3 fusion.139
  293.8 1.3 fusion.140
  295.1 1.3 fusion.139
  298.7 1.3 fusion.140
  300.0 1.3 fusion.139
  303.5 1.3 fusion.140
  304.9 1.3 fusion.139
  308.4 1.3 fusion.140
  309.8 1.3 fusion.139
  313.3 1.3 fusion.140
  314.6 1.3 fusion.139
  318.2 1.3 fusion.140
  319.5 1.3 fusion.139
  323.1 1.3 fusion.140
  324.4 1.3 fusion.139
  328.0 1.3 fusion.140
  329.3 1.3 fusion.139
  332.8 1.3 fusion.140
  334.2 1.3 fusion.139
  336.2 25.0 %all_to_all.25 = bf16[8,32,2048]{2,1,0:T(8,128)(2,1)S(1)} all-to-all(bf16[8,32,2048]{2,1,0:T(8,128)(2,1)S(1)} %bitcast.183), channel_id=1, replica_groups=mesh['sp'=64,'tp'=8] {'tp'}, dimensions={0} | all-to-all | bytes 2097152 | tf_op jit(solution)/shard_map/all_to_all | solution.py:49
  (229 shorter events, 44.3 us)
Async XLA Ops:
  6.5 329.1 %copy-start = (bf16[128,2048]{1,0:T(8,128)(2,1)S(1)}, bf16[128,2048]{1,0:T(8,128)(2,1)}, u32[]{:S(2)}) copy-start(bf16[128,2048]{1,0:T(8,128)(2,1)} %param.29) | copy-start | bytes 1572868
  6.5 63.0 %copy-start.3 = (bf16[2048,64]{0,1:T(8,128)(2,1)S(1)}, bf16[2048,64]{0,1:T(8,128)(2,1)}, u32[]{:S(2)}) copy-start(bf16[2048,64]{0,1:T(8,128)(2,1)} %param.23) | copy-start | bytes 786436
  6.5 63.5 %copy-start.4 = (bf16[2048,64]{0,1:T(8,128)(2,1)S(1)}, bf16[2048,64]{0,1:T(8,128)(2,1)}, u32[]{:S(2)}) copy-start(bf16[2048,64]{0,1:T(8,128)(2,1)} %param.24) | copy-start | bytes 786436
  6.5 64.7 %copy-start.1 = (bf16[2048,128]{1,0:T(8,128)(2,1)S(1)}, bf16[2048,128]{1,0:T(8,128)(2,1)}, u32[]{:S(2)}) copy-start(bf16[2048,128]{1,0:T(8,128)(2,1)} %param.25) | copy-start | bytes 1572868
  8.2 14.7 %all-to-all-start = ((f32[8,2,96]{2,1,0:T(2,128)}), f32[8,2,96]{2,1,0:T(2,128)S(1)}, u32[]{:S(2)}, u32[]{:S(2)}) async-start(f32[8,2,96]{2,1,0:T(2,128)} %broadcast_in_dim.22), calls=%async_computation | async-start | bytes 16384 | tf_op jit(solution)/shard_map/all_to_all | solution.py:16
  23.6 23.1 %all-to-all-start.1 = ((f32[64,2,96]{2,1,0:T(2,128)}), f32[64,2,96]{2,1,0:T(2,128)S(1)}, u32[]{:S(2)}, u32[]{:S(2)}) async-start(f32[64,2,96]{2,1,0:T(2,128)} %broadcast_in_dim.23), calls=%async_computation.1 | async-start | bytes 131072 | tf_op jit(solution)/shard_map/all_to_all | solution.py:16
  49.0 20.6 %all-to-all-start.2 = ((bf16[8,32,2048]{2,1,0:T(8,128)(2,1)}), bf16[8,32,2048]{2,1,0:T(8,128)(2,1)S(1)}, u32[]{:S(2)}, u32[]{:S(2)}) async-start(bf16[8,32,2048]{2,1,0:T(8,128)(2,1)} %broadcast_in_dim.25), calls=%async_computation.2 | async-start | bytes 2097152 | tf_op jit(solution)/shard_map/all_to_all | solution.py:16
  54.6 196.4 %all-gather.2.cloned.1.call-start = ((), (), s32[]{:S(2)}) async-start(), calls=%async_computation.5 | async-start | bytes 4259840 | tf_op jit(solution)/shard_map/all_gather | solution.py:190
  74.6 7.1 %copy-start.7 = (bf16[8,2048]{1,0:T(8,128)(2,1)S(1)}, bf16[8,2048]{1,0:T(8,128)(2,1)}, u32[]{:S(2)}) copy-start(bf16[8,2048]{1,0:T(8,128)(2,1)} %param.17) | copy-start | bytes 98308
  74.6 168.7 %copy-start.5 = (bf16[2048,64]{0,1:T(8,128)(2,1)S(1)}, bf16[2048,64]{0,1:T(8,128)(2,1)}, u32[]{:S(2)}) copy-start(bf16[2048,64]{0,1:T(8,128)(2,1)} %param.22) | copy-start | bytes 786436
  74.6 169.2 %copy-start.6 = (bf16[2048,64]{0,1:T(8,128)(2,1)S(1)}, bf16[2048,64]{0,1:T(8,128)(2,1)}, u32[]{:S(2)}) copy-start(bf16[2048,64]{0,1:T(8,128)(2,1)} %param.21) | copy-start | bytes 786436
  74.6 182.8 %all-to-all-start.3 = ((bf16[64,256,128]{2,1,0:T(8,128)(2,1)}), bf16[64,256,128]{2,1,0:T(8,128)(2,1)}, u32[]{:S(2)}, u32[]{:S(2)}) async-start(bf16[64,256,128]{2,1,0:T(8,128)(2,1)} %stack.11), calls=%async_computation.3 | async-start | bytes 8388608 | tf_op jit(solution)/shard_map/all_to_all | solution.py:192
  257.4 78.2 %copy-start.8 = (f32[128]{0:T(128)S(1)}, f32[128]{0:T(128)}, u32[]{:S(2)}) copy-start(f32[128]{0:T(128)} %param.28) | copy-start | bytes 1540
  335.5 25.8 %copy-start.2 = (bf16[32,2048]{1,0:T(8,128)(2,1)S(1)}, bf16[32,2048]{1,0:T(8,128)(2,1)}, u32[]{:S(2)}) copy-start(bf16[32,2048]{1,0:T(8,128)(2,1)} %param.16) | copy-start | bytes 393220
Sparse Core Ops, SparseCore 0:
  71.3 179.6 all-gather.1
